TPU v7x, 32 devices: a whole 2x2x4 slice. The times are simulated.
32 devices in a mesh: sp: 8 (over z, x), tp: 4 (over y, core).
Axes of the slice: x: 2, y: 2, z: 4, core: 2. Of those that a mesh axis runs over, the one named last changes fastest.
Arguments:
- queries: bfloat16 [2048, 1024], P('sp', 'tp'), may hold values from -6 to 6
- keys: bfloat16 [2048, 1024], P('sp', 'tp'), may hold values from -6 to 6
- values: bfloat16 [2048, 2048], P('sp', 'tp'), may hold values from -6 to 6
- gate_code: bfloat16 [2048, 32], P('sp'), may hold values from -5.5 to 5.5
- gate_up: bfloat16 [32, 1024], P(None, 'tp'), may hold values from -1 to 1
- gate_bias: float32 [1024], P('tp'), as said below
- gla_gain: float32 [256], replicated, may hold values from 0.1 to 1.9
- conv_input: bfloat16 [2048, 2048], P('sp', 'tp'), may hold values from -6 to 6
- conv_gate: bfloat16 [2048, 2048], P('sp', 'tp'), may hold values from -6 to 6
- conv_taps: float32 [3, 2048], P(None, 'tp'), may hold values from -3.5 to 3.5
- out_gla: bfloat16 [2048, 2048], P('tp', 'sp'), may hold values from -0.09375 to 0.09375
- out_conv: bfloat16 [2048, 2048], P('tp', 'sp'), may hold values from -0.09375 to 0.09375
Outputs:
- mixed: bfloat16 [2048, 2048], P(('sp', 'tp'))
Inputs may be any that keep to these rules, and one draw needn't show every extreme that they name: `gate_bias`: every bias is at least 1.5, so every decay per step lies strictly between 0 and 1.
All inputs are finite; a program needn't handle non-finite values.
Results may differ from a plain program's by a relative error of at most 0.028.
Values may be sent and summed in bfloat16 or wider, within the bound.
A program may use at most 64 MiB of HBM per device.

v0:
```python
import jax
import jax.numpy as jnp
from jax import lax
from jax.sharding import PartitionSpec as P

KEY_WIDTH = 128
HEAD_V = 256
SEGMENT_LENGTH = 64
softness_divisor = 16.0
epsilon = 1.0


def for_sending(x):
    return jax.tree.map(lambda a: a.astype(jnp.bfloat16) if a.dtype == jnp.float32 else a, x)


def from_behind(x, axis, by):
    count = lax.axis_size(axis)
    pairs = [(i, i + by) for i in range(count) if 0 <= i + by < count]
    return lax.ppermute(x, axis, pairs)


def chain(earlier, latter):
    return (earlier[0] * latter[0], latter[0][..., None] * earlier[1] + latter[1])


def per_device(
    queries,
    keys,
    values,
    gate_code,
    gate_up,
    gate_bias,
    gla_gain,
    conv_input,
    conv_gate,
    conv_taps,
    out_gla,
    out_conv,
):
    row_count = queries.shape[0]
    segment_count = row_count // SEGMENT_LENGTH
    head_count = queries.shape[1] // KEY_WIDTH
    gate_score = jnp.dot(gate_code, gate_up, preferred_element_type=jnp.float32) + gate_bias
    decay_logarithm = (jax.nn.log_sigmoid(gate_score) / softness_divisor).reshape(
        segment_count, SEGMENT_LENGTH, head_count, KEY_WIDTH
    )
    inside = jnp.cumsum(decay_logarithm, axis=1)
    seg_total = inside[:, -1]
    key_blocks = keys.reshape(segment_count, SEGMENT_LENGTH, head_count, KEY_WIDTH)
    scaled_keys = (key_blocks * jnp.exp(seg_total[:, None] - inside)).astype(jnp.bfloat16)
    value_blocks = values.reshape(segment_count, SEGMENT_LENGTH, head_count, HEAD_V)
    update = jnp.einsum(
        "nshk,nshv->nhkv", scaled_keys, value_blocks, preferred_element_type=jnp.float32
    )
    through, local_state = lax.associative_scan(chain, (jnp.exp(seg_total), update), axis=0)
    device_decay = through[-1]
    device_state = local_state[-1]
    columns = lax.all_to_all(
        device_state[None].astype(jnp.bfloat16), "sp", split_axis=3, concat_axis=0, tiled=True
    ).astype(jnp.float32)
    decays = lax.all_gather(device_decay[None], "sp", axis=0, tiled=True)
    running = lax.associative_scan(chain, (decays, columns), axis=0)[1]
    before = jnp.concatenate([jnp.zeros_like(running[:1]), running[:-1]], axis=0)
    incoming = lax.all_to_all(
        for_sending(before), "sp", split_axis=0, concat_axis=3, tiled=True
    ).astype(before.dtype)[0]
    states = local_state + through[..., None] * incoming[None]
    query_blocks = queries.reshape(segment_count, SEGMENT_LENGTH, head_count, KEY_WIDTH)
    readout = jnp.einsum(
        "nshk,nhkv->nshv",
        query_blocks,
        states.astype(jnp.bfloat16),
        preferred_element_type=jnp.float32,
    )
    norm_scale = lax.rsqrt(jnp.mean(readout * readout, axis=-1, keepdims=True) + epsilon)
    gla_mix = (
        (readout * norm_scale * gla_gain)
        .astype(jnp.bfloat16)
        .reshape(row_count, head_count * HEAD_V)
    )
    reach_rows = conv_taps.shape[0] - 1
    earlier_rows = from_behind(conv_input[row_count - reach_rows :], "sp", 1)
    extended = jnp.concatenate([earlier_rows, conv_input], axis=0)
    convolved = jnp.zeros(conv_input.shape, jnp.float32)
    for offset in range(reach_rows + 1):
        convolved = convolved + conv_taps[offset] * extended[offset : offset + row_count]
    conv_mix = (conv_gate * convolved).astype(jnp.bfloat16)
    wide_gla, wide_conv = (
        lax.all_gather(out_gla, "sp", axis=1, tiled=True),
        lax.all_gather(out_conv, "sp", axis=1, tiled=True),
    )
    summed = jnp.dot(gla_mix, wide_gla, preferred_element_type=jnp.float32)
    return lax.psum_scatter(
        (summed + jnp.dot(conv_mix, wide_conv, preferred_element_type=jnp.float32)).astype(
            jnp.bfloat16
        ),
        "tp",
        scatter_dimension=0,
        tiled=True,
    )


def solution(mesh):
    in_specs = (
        P("sp", "tp"),
        P("sp", "tp"),
        P("sp", "tp"),
        P("sp", None),
        P(None, "tp"),
        P("tp"),
        P(),
        P("sp", "tp"),
        P("sp", "tp"),
        P(None, "tp"),
        P("tp", "sp"),
        P("tp", "sp"),
    )
    out_specs = P(("sp", "tp"), None)
    return jax.shard_map(
        per_device, mesh=mesh, in_specs=in_specs, out_specs=out_specs, check_vma=False
    )
```

profile of v0, /device:TPU:0, one launch (start us, length us, event | category | flops | bytes accessed | tf_op | source)
XLA Modules:
  0.0 149.3 jit_solution(18421803840476476254)
XLA Ops:
  6.5 0.7 all-gather.3.cloned.1.call-update
  7.3 1.1 fusion.9
  8.3 0.1 reshape.57
  8.5 1.0 reshape.61
  9.8 0.2 multiply_convert_fusion.3
  10.0 0.3 fusion.11
  11.1 0.8 copy.32
  11.9 7.3 %all-to-all-start = ((bf16[1,2,128,256]{2,1,0,3:T(2,128)(2,1)}), bf16[1,2,128,256]{2,1,0,3:T(2,128)(2,1)S(1)}, u32[]{:S(2)}, u32[]{:S(2)}) async-start(bf16[1,2,128,256]{2,1,0,3:T(2,128)(2,1)} %copy.32), calls=%async_computation | async-start | bytes 262144 | tf_op jit(solution)/shard_map/all_to_all | solution.py:59
  19.2 0.7 all-gather.5.cloned.1.call-update
  20.0 21.3 %all_gather.9 = f32[8,2,128]{2,1,0:T(2,128)S(1)} all-gather(f32[1,2,128]{2,1,0:T(2,128)S(1)} %slice_add_fusion.5), channel_id=1, replica_groups=mesh['sp'=8,'tp'=4] {'sp'}, dimensions={0}, use_global_device_ids=true | all-gather | bytes 9216 | tf_op jit(solution)/shard_map/all_gather | solution.py:62
  41.4 0.6 copy.35
  42.5 0.7 fusion.18
  43.4 0.7 concatenate.22.clone
  44.1 3.4 %all-to-all-start.1 = ((bf16[8,2,128,32]{2,3,1,0:T(8,128)(2,1)}), bf16[8,2,128,32]{2,3,1,0:T(8,128)(2,1)S(1)}, u32[]{:S(2)}, u32[]{:S(2)}) async-start(bf16[8,2,128,32]{2,3,1,0:T(8,128)(2,1)} %concatenate.22.clone), calls=%async_computation.1 | async-start | bytes 262144 | tf_op jit(solution)/shard_map/all_to_all | solution.py:65
  47.5 3.8 %collective-permute-start = (bf16[2,512]{1,0:T(2,128)(2,1)S(1)}, bf16[2,512]{1,0:T(2,128)(2,1)S(1)}, u32[]{:S(2)}, u32[]{:S(2)}) collective-permute-start(bf16[2,512]{1,0:T(2,128)(2,1)S(1)} %slice.187), channel_id=1, source_target_pairs={{0,4},{4,8},{8,12},{12,16},{16,20},{20,24},{24,28},{1,5},{5,9},{9,... | collective-permute-start | bytes 6152 | tf_op jit(solution)/shard_map/ppermute | solution.py:20
  51.4 5.2 %all-to-all-done.1 = bf16[8,2,128,32]{2,3,1,0:T(8,128)(2,1)S(1)} async-done(((bf16[8,2,128,32]{2,3,1,0:T(8,128)(2,1)}), bf16[8,2,128,32]{2,3,1,0:T(8,128)(2,1)S(1)}, u32[]{:S(2)}, u32[]{:S(2)}) %all-to-all-start.1) | async-done | bytes 131104 | tf_op jit(solution)/shard_map/all_to_all | solution.py:65
  56.8 0.5 multiply_reduce_fusion
  57.3 0.1 multiply_convert_fusion.1
  57.4 0.3 copy.42
  57.7 8.6 %all-gather.3.cloned.1.call-done = bf16[512,2048]{1,0:T(8,128)(2,1)} async-done(((bf16[512,256]{1,0:T(8,128)(2,1)}), bf16[512,2048]{1,0:T(8,128)(2,1)}) %all-gather.3.cloned.1.call-update) | async-done | bytes 2097168 | tf_op jit(solution)/shard_map/all_gather | solution.py:90
  66.3 2.3 %fusion.34 = f32[256,2048]{1,0:T(8,128)S(1)} fusion(bf16[256,512]{1,0:T(8,128)(2,1)S(1)} %bitcast.43, bf16[512,2048]{1,0:T(8,128)(2,1)} %all-gather.3.cloned.1.call-done), kind=kOutput, calls=%fused_computation.81 | convolution fusion | flops 536870912 | bytes 4456448 | tf_op jit(solution)/shard_map/dot_general | solution.py:93
  68.7 47.5 %all-gather.5.cloned.1.call-done = bf16[512,2048]{1,0:T(8,128)(2,1)} async-done(((bf16[512,256]{1,0:T(8,128)(2,1)}), bf16[512,2048]{1,0:T(8,128)(2,1)}) %all-gather.5.cloned.1.call-update) | async-done | bytes 2097168 | tf_op jit(solution)/shard_map/all_gather | solution.py:91
  116.2 3.4 %fusion = bf16[256,2048]{1,0:T(8,128)(2,1)} fusion(f32[256,2048]{1,0:T(8,128)S(1)} %fusion.34, bf16[512,2048]{1,0:T(8,128)(2,1)} %all-gather.5.cloned.1.call-done, bf16[256,512]{1,0:T(8,128)(2,1)S(1)} %copy-done.1, bf16[256,512]{1,0:T(8,128)(2,1)S(1)} %copy-done.2, bf16[2,512]{1,0:T(2,128)(2,1)S(1)} %collective-permute-done, f32[512]{0:T(512)S(1)} %bitcast.48, ...), kind=kOutput, calls=%fused_computation.1 | convolution fusion | flops 540147712 | bytes 5775360 | tf_op jit(solution)/shard_map/dot_general | solution.py:95
  119.6 23.1 %reduce-scatter.2.cloned.1.call-done = bf16[64,2048]{1,0:T(8,128)(2,1)} async-done(((bf16[256,2048]{1,0:T(8,128)(2,1)}), bf16[64,2048]{1,0:T(8,128)(2,1)}) %reduce-scatter.2.cloned.1.call-update) | async-done | bytes 262160 | tf_op jit(solution)/shard_map/reduce_scatter | solution.py:94
  (80 shorter events, 1.9 us)
Async XLA Ops:
  6.5 0.7 copy-start
  6.5 3.0 %copy-start.3 = (bf16[256,512]{1,0:T(8,128)(2,1)S(1)}, bf16[256,512]{1,0:T(8,128)(2,1)}, u32[]{:S(2)}) copy-start(bf16[256,512]{1,0:T(8,128)(2,1)} %param.14) | copy-start | bytes 786436
  6.5 59.8 %all-gather.3.cloned.1.call-start = ((), (), s32[]{:S(2)}) async-start(), calls=%async_computation.3 | async-start | bytes 2359296 | tf_op jit(solution)/shard_map/all_gather | solution.py:90
  11.9 30.1 %all-to-all-start = ((bf16[1,2,128,256]{2,1,0,3:T(2,128)(2,1)}), bf16[1,2,128,256]{2,1,0,3:T(2,128)(2,1)S(1)}, u32[]{:S(2)}, u32[]{:S(2)}) async-start(bf16[1,2,128,256]{2,1,0,3:T(2,128)(2,1)} %copy.32), calls=%async_computation | async-start | bytes 262144 | tf_op jit(solution)/shard_map/all_to_all | solution.py:59
  19.1 97.1 %all-gather.5.cloned.1.call-start = ((), (), s32[]{:S(2)}) async-start(), calls=%async_computation.4 | async-start | bytes 2359296 | tf_op jit(solution)/shard_map/all_gather | solution.py:91
  19.9 22.1 %copy-start.5 = (f32[4,2,128]{2,1,0:T(2,128)}, f32[4,2,128]{2,1,0:T(2,128)S(1)}, u32[]{:S(2)}) copy-start(f32[4,2,128]{2,1,0:T(2,128)S(1)} %pad.53) | copy-start | bytes 12292
  20.0 22.0 %copy-start.7 = (f32[4,2,128]{2,1,0:T(2,128)}, f32[4,2,128]{2,1,0:T(2,128)S(1)}, u32[]{:S(2)}) copy-start(f32[4,2,128]{2,1,0:T(2,128)S(1)} %pad.54) | copy-start | bytes 12292
  42.1 5.4 %copy-start.1 = (bf16[256,512]{1,0:T(8,128)(2,1)S(1)}, bf16[256,512]{1,0:T(8,128)(2,1)}, u32[]{:S(2)}) copy-start(bf16[256,512]{1,0:T(8,128)(2,1)} %param.19) | copy-start | bytes 786436
  42.4 8.9 %copy-start.4 = (bf16[256,256]{1,0:T(8,128)(2,1)S(1)}, bf16[256,256]{1,0:T(8,128)(2,1)}, u32[]{:S(2)}) copy-start(bf16[256,256]{1,0:T(8,128)(2,1)} %param.12) | copy-start | bytes 393220
  42.5 8.9 %copy-start.6 = (f32[4,2,128]{2,1,0:T(2,128)S(1)}, f32[4,2,128]{2,1,0:T(2,128)}, u32[]{:S(2)}) copy-start(f32[4,2,128]{2,1,0:T(2,128)} %copy-done.5) | copy-start | bytes 12292
  42.5 8.9 %copy-start.8 = (f32[4,2,128]{2,1,0:T(2,128)S(1)}, f32[4,2,128]{2,1,0:T(2,128)}, u32[]{:S(2)}) copy-start(f32[4,2,128]{2,1,0:T(2,128)} %copy-done.7) | copy-start | bytes 12292
  42.5 8.9 %copy-start.9 = (f32[3,512]{1,0:T(4,128)S(1)}, f32[3,512]{1,0:T(4,128)}, u32[]{:S(2)}) copy-start(f32[3,512]{1,0:T(4,128)} %param.21) | copy-start | bytes 18436
  44.1 12.6 %all-to-all-start.1 = ((bf16[8,2,128,32]{2,3,1,0:T(8,128)(2,1)}), bf16[8,2,128,32]{2,3,1,0:T(8,128)(2,1)S(1)}, u32[]{:S(2)}, u32[]{:S(2)}) async-start(bf16[8,2,128,32]{2,3,1,0:T(8,128)(2,1)} %concatenate.22.clone), calls=%async_computation.1 | async-start | bytes 262144 | tf_op jit(solution)/shard_map/all_to_all | solution.py:65
  47.5 95.3 %reduce-scatter.2.cloned.1.call-start = ((), (), s32[]{:S(2)}) async-start(), calls=%async_computation.5 | async-start | bytes 1310720 | tf_op jit(solution)/shard_map/reduce_scatter | solution.py:94
  47.5 21.1 %collective-permute-start = (bf16[2,512]{1,0:T(2,128)(2,1)S(1)}, bf16[2,512]{1,0:T(2,128)(2,1)S(1)}, u32[]{:S(2)}, u32[]{:S(2)}) collective-permute-start(bf16[2,512]{1,0:T(2,128)(2,1)S(1)} %slice.187), channel_id=1, source_target_pairs={{0,4},{4,8},{8,12},{12,16},{16,20},{20,24},{24,28},{1,5},{5,9},{9,... | collective-permute-start | bytes 6152 | tf_op jit(solution)/shard_map/ppermute | solution.py:20
  51.4 5.9 %copy-start.10 = (f32[256]{0:T(256)S(1)}, f32[256]{0:T(256)}, u32[]{:S(2)}) copy-start(f32[256]{0:T(256)} %param.18) | copy-start | bytes 3076
  66.3 49.9 %copy-start.2 = (bf16[256,512]{1,0:T(8,128)(2,1)S(1)}, bf16[256,512]{1,0:T(8,128)(2,1)}, u32[]{:S(2)}) copy-start(bf16[256,512]{1,0:T(8,128)(2,1)} %param.20) | copy-start | bytes 786436
Sparse Core Ops, SparseCore 0:
  9.4 56.8 all-gather.2
  68.4 47.8 all-gather.4
  119.7 22.9 reduce-scatter.1
where the time goes:
time: 150 us; the launch traced here: 149 us
  waiting for transfers between devices  85.9 us (57%)
  blocking collectives  21.3 us (14%)
  starting transfers between devices  14.5 us (10%)
  between operations  13.7 us (9%)
  matrix products  7.61 us (5%)
  local copies, waits for them, and re-layouts  4.46 us (3%)
  other arithmetic  1.88 us (1%)
    all_gather x1, waiting for transfers between devices, per_device(): lax.all_gather(out_conv, 'sp', axis=1, tiled=True)  47.5 us
    reduce_scatter x1, waiting for transfers between devices, per_device(): lax.psum_scatter((summed + jnp.dot(conv_mix, wide_conv, preferred_element...  23.1 us
    all_gather x1, blocking collectives, per_device(): decays = lax.all_gather(device_decay[None], 'sp', axis=0, tiled=True)  21.3 us
    all_gather x1, waiting for transfers between devices, per_device(): lax.all_gather(out_gla, 'sp', axis=1, tiled=True)  8.57 us
    all_to_all x1, starting transfers between devices, per_device(): lax.all_to_all(device_state[None].astype(jnp.bfloat16), 'sp', split_axis=...  7.28 us
    all_to_all x1, waiting for transfers between devices, per_device(): lax.all_to_all(for_sending(before), 'sp', split_axis=0, concat_axis=3, ti...  5.2 us
    ppermute x1, starting transfers between devices, from_behind(): return lax.ppermute(x, axis, pairs)  3.77 us
    dot_general x1, matrix products, per_device(): jnp.dot(conv_mix, wide_conv, preferred_element_type=jnp.float32)  3.39 us
  transfers between devices with their start and end apart: 6, of which 4 were waited for; matrix products, arithmetic and copies ran while one was open for 7% of the time, Pallas kernels for 0%

commit v1 on v0

--- a/solution.py
+++ b/solution.py
@@ -62,8 +62,11 @@
     decays = lax.all_gather(device_decay[None], "sp", axis=0, tiled=True)
     running = lax.associative_scan(chain, (decays, columns), axis=0)[1]
     before = jnp.concatenate([jnp.zeros_like(running[:1]), running[:-1]], axis=0)
-    incoming = lax.all_to_all(
-        for_sending(before), "sp", split_axis=0, concat_axis=3, tiled=True
+    incoming = jnp.concatenate(
+        lax.all_to_all(
+            jnp.stack(jnp.split(for_sending(before), lax.axis_size("sp"), axis=0)), "sp", 0, 0
+        ),
+        axis=3,
     ).astype(before.dtype)[0]
     states = local_state + through[..., None] * incoming[None]
     query_blocks = queries.reshape(segment_count, SEGMENT_LENGTH, head_count, KEY_WIDTH)

time: 150 us -> 152 us (1.013)
  local copies, waits for them, and re-layouts: 4.46 us -> 8.67 us
  waiting for transfers between devices: 85.9 us -> 83 us
    all_gather x1, waiting for transfers between devices: 8.57 us -> 4.37 us  [per_device(): lax.all_gather(out_gla, 'sp', axis=1, tiled=True)]
    unnamed x25 -> x26, local copies, waits for them, and re-layouts: 0.19 us -> 4.35 us
    all_gather x1, waiting for transfers between devices: 47.5 us -> 50.6 us  [per_device(): lax.all_gather(out_conv, 'sp', axis=1, tiled=True)]
    all_to_all x1, waiting for transfers between devices: 5.2 us -> 3.41 us  [per_device(): lax.all_to_all(jnp.stack(jnp.split(for_sending(before), lax.axis_size('sp...]
  transfers between devices with their start and end apart: 6 -> 6, of which waited for: 4 -> 4; matrix products, arithmetic and copies ran while one was open for 7% -> 10% of each run, Pallas kernels for 0% -> 0%
where the time goes in v1:
time: 152 us; the launch traced here: 151 us
  waiting for transfers between devices  83 us (55%)
  blocking collectives  21.3 us (14%)
  starting transfers between devices  14.5 us (10%)
  between operations  13.6 us (9%)
  local copies, waits for them, and re-layouts  8.67 us (6%)
  matrix products  7.63 us (5%)
  other arithmetic  2.55 us (2%)
    all_gather x1, waiting for transfers between devices, per_device(): lax.all_gather(out_conv, 'sp', axis=1, tiled=True)  50.6 us
    reduce_scatter x1, waiting for transfers between devices, per_device(): lax.psum_scatter((summed + jnp.dot(conv_mix, wide_conv, preferred_element...  23.1 us
    all_gather x1, blocking collectives, per_device(): decays = lax.all_gather(device_decay[None], 'sp', axis=0, tiled=True)  21.3 us
    all_to_all x1, starting transfers between devices, per_device(): lax.all_to_all(device_state[None].astype(jnp.bfloat16), 'sp', split_axis=...  7.28 us
    all_gather x1, waiting for transfers between devices, per_device(): lax.all_gather(out_gla, 'sp', axis=1, tiled=True)  4.37 us
    unnamed x26, local copies, waits for them, and re-layouts  4.35 us
    ppermute x1, starting transfers between devices, from_behind(): return lax.ppermute(x, axis, pairs)  3.77 us
    dot_general x1, matrix products, per_device(): jnp.dot(conv_mix, wide_conv, preferred_element_type=jnp.float32)  3.42 us
  transfers between devices with their start and end apart: 6, of which 4 were waited for; matrix products, arithmetic and copies ran while one was open for 10% of the time, Pallas kernels for 0%

profile of v1, /device:TPU:0, one launch (start us, length us, event | category | flops | bytes accessed | tf_op | source)
XLA Modules:
  0.0 151.2 jit_solution(9573472055956445038)
XLA Ops:
  6.5 0.7 all-gather.3.cloned.1.call-update
  7.3 1.1 fusion.9
  8.5 1.0 reshape.61
  11.1 0.8 copy.45
  11.9 7.3 %all-to-all-start = ((bf16[1,2,128,256]{2,1,0,3:T(2,128)(2,1)}), bf16[1,2,128,256]{2,1,0,3:T(2,128)(2,1)S(1)}, u32[]{:S(2)}, u32[]{:S(2)}) async-start(bf16[1,2,128,256]{2,1,0,3:T(2,128)(2,1)} %copy.45), calls=%async_computation | async-start | bytes 262144 | tf_op jit(solution)/shard_map/all_to_all | solution.py:59
  19.2 0.7 all-gather.5.cloned.1.call-update
  20.0 21.3 %all_gather.9 = f32[8,2,128]{2,1,0:T(2,128)S(1)} all-gather(f32[1,2,128]{2,1,0:T(2,128)S(1)} %slice_add_fusion.5), channel_id=1, replica_groups=mesh['sp'=8,'tp'=4] {'sp'}, dimensions={0}, use_global_device_ids=true | all-gather | bytes 9216 | tf_op jit(solution)/shard_map/all_gather | solution.py:62
  41.3 0.6 constant_dynamic-update-slice_fusion.7
  43.0 0.7 fusion.18
  44.0 0.6 constant_dynamic-update-slice_fusion.6
  44.6 0.6 constant_dynamic-update-slice_fusion.5
  45.2 0.6 constant_dynamic-update-slice_fusion.4
  45.8 0.6 constant_dynamic-update-slice_fusion.3
  46.4 0.6 constant_dynamic-update-slice_fusion.2
  47.0 0.6 constant_dynamic-update-slice_fusion.1
  48.2 3.4 %all-to-all-start.1 = ((bf16[8,1,2,128,32]{3,4,2,1,0:T(8,128)(2,1)}), bf16[8,1,2,128,32]{3,4,2,1,0:T(8,128)(2,1)S(1)}, u32[]{:S(2)}, u32[]{:S(2)}) async-start(bf16[8,1,2,128,32]{3,4,2,1,0:T(8,128)(2,1)} %constant_dynamic-update-slice_fusion), calls=%async_computation.1 | async-start | bytes 262144 | tf_op jit(solution)/shard_map/all_to_all | solution.py:66
  51.7 3.8 %collective-permute-start = (bf16[2,512]{1,0:T(2,128)(2,1)S(1)}, bf16[2,512]{1,0:T(2,128)(2,1)S(1)}, u32[]{:S(2)}, u32[]{:S(2)}) collective-permute-start(bf16[2,512]{1,0:T(2,128)(2,1)S(1)} %slice.198), channel_id=1, source_target_pairs={{0,4},{4,8},{8,12},{12,16},{16,20},{20,24},{24,28},{1,5},{5,9},{9,... | collective-permute-start | bytes 6152 | tf_op jit(solution)/shard_map/ppermute | solution.py:20
  55.4 0.7 add.120
  56.2 3.4 %all-to-all-done.1 = bf16[8,1,2,128,32]{3,4,2,1,0:T(8,128)(2,1)S(1)} async-done(((bf16[8,1,2,128,32]{3,4,2,1,0:T(8,128)(2,1)}), bf16[8,1,2,128,32]{3,4,2,1,0:T(8,128)(2,1)S(1)}, u32[]{:S(2)}, u32[]{:S(2)}) %all-to-all-start.1) | async-done | bytes 131104 | tf_op jit(solution)/shard_map/all_to_all | solution.py:66
  60.8 4.4 %all-gather.3.cloned.1.call-done = bf16[512,2048]{1,0:T(8,128)(2,1)} async-done(((bf16[512,256]{1,0:T(8,128)(2,1)}), bf16[512,2048]{1,0:T(8,128)(2,1)}) %all-gather.3.cloned.1.call-update) | async-done | bytes 2097168 | tf_op jit(solution)/shard_map/all_gather | solution.py:93
  65.2 2.3 %fusion.34 = f32[256,2048]{1,0:T(8,128)S(1)} fusion(bf16[256,512]{1,0:T(8,128)(2,1)S(1)} %bitcast.78, bf16[512,2048]{1,0:T(8,128)(2,1)} %all-gather.3.cloned.1.call-done), kind=kOutput, calls=%fused_computation.96 | convolution fusion | flops 536870912 | bytes 4456448 | tf_op jit(solution)/shard_map/dot_general | solution.py:96
  67.5 50.6 %all-gather.5.cloned.1.call-done = bf16[512,2048]{1,0:T(8,128)(2,1)} async-done(((bf16[512,256]{1,0:T(8,128)(2,1)}), bf16[512,2048]{1,0:T(8,128)(2,1)}) %all-gather.5.cloned.1.call-update) | async-done | bytes 2097168 | tf_op jit(solution)/shard_map/all_gather | solution.py:94
  118.2 3.4 %fusion = bf16[256,2048]{1,0:T(8,128)(2,1)} fusion(f32[256,2048]{1,0:T(8,128)S(1)} %fusion.34, bf16[512,2048]{1,0:T(8,128)(2,1)} %all-gather.5.cloned.1.call-done, bf16[256,512]{1,0:T(8,128)(2,1)S(1)} %copy-done.1, bf16[256,512]{1,0:T(8,128)(2,1)S(1)} %copy-done.2, bf16[2,512]{1,0:T(2,128)(2,1)S(1)} %collective-permute-done, f32[512]{0:T(512)S(1)} %bitcast.83, ...), kind=kOutput, calls=%fused_computation.1 | convolution fusion | flops 540147712 | bytes 5775360 | tf_op jit(solution)/shard_map/dot_general | solution.py:98
  121.6 23.1 %reduce-scatter.2.cloned.1.call-done = bf16[64,2048]{1,0:T(8,128)(2,1)} async-done(((bf16[256,2048]{1,0:T(8,128)(2,1)}), bf16[64,2048]{1,0:T(8,128)(2,1)}) %reduce-scatter.2.cloned.1.call-update) | async-done | bytes 262160 | tf_op jit(solution)/shard_map/reduce_scatter | solution.py:97
  (83 shorter events, 4.6 us)
Async XLA Ops:
  6.5 0.7 copy-start
  6.5 3.0 %copy-start.3 = (bf16[256,512]{1,0:T(8,128)(2,1)S(1)}, bf16[256,512]{1,0:T(8,128)(2,1)}, u32[]{:S(2)}) copy-start(bf16[256,512]{1,0:T(8,128)(2,1)} %param.14) | copy-start | bytes 786436
  6.5 58.6 %all-gather.3.cloned.1.call-start = ((), (), s32[]{:S(2)}) async-start(), calls=%async_computation.3 | async-start | bytes 2359296 | tf_op jit(solution)/shard_map/all_gather | solution.py:93
  11.9 30.7 %all-to-all-start = ((bf16[1,2,128,256]{2,1,0,3:T(2,128)(2,1)}), bf16[1,2,128,256]{2,1,0,3:T(2,128)(2,1)S(1)}, u32[]{:S(2)}, u32[]{:S(2)}) async-start(bf16[1,2,128,256]{2,1,0,3:T(2,128)(2,1)} %copy.45), calls=%async_computation | async-start | bytes 262144 | tf_op jit(solution)/shard_map/all_to_all | solution.py:59
  19.1 99.0 %all-gather.5.cloned.1.call-start = ((), (), s32[]{:S(2)}) async-start(), calls=%async_computation.4 | async-start | bytes 2359296 | tf_op jit(solution)/shard_map/all_gather | solution.py:94
  19.9 22.6 %copy-start.5 = (f32[4,2,128]{2,1,0:T(2,128)}, f32[4,2,128]{2,1,0:T(2,128)S(1)}, u32[]{:S(2)}) copy-start(f32[4,2,128]{2,1,0:T(2,128)S(1)} %pad.53) | copy-start | bytes 12292
  20.0 22.6 %copy-start.6 = (f32[4,2,128]{2,1,0:T(2,128)}, f32[4,2,128]{2,1,0:T(2,128)S(1)}, u32[]{:S(2)}) copy-start(f32[4,2,128]{2,1,0:T(2,128)S(1)} %pad.54) | copy-start | bytes 12292
  42.7 9.0 %copy-start.1 = (bf16[256,512]{1,0:T(8,128)(2,1)S(1)}, bf16[256,512]{1,0:T(8,128)(2,1)}, u32[]{:S(2)}) copy-start(bf16[256,512]{1,0:T(8,128)(2,1)} %param.19) | copy-start | bytes 786436
  43.0 13.1 %copy-start.4 = (bf16[256,256]{1,0:T(8,128)(2,1)S(1)}, bf16[256,256]{1,0:T(8,128)(2,1)}, u32[]{:S(2)}) copy-start(bf16[256,256]{1,0:T(8,128)(2,1)} %param.12) | copy-start | bytes 393220
  43.8 12.4 %copy-start.7 = (f32[3,512]{1,0:T(4,128)S(1)}, f32[3,512]{1,0:T(4,128)}, u32[]{:S(2)}) copy-start(f32[3,512]{1,0:T(4,128)} %param.21) | copy-start | bytes 18436
  48.2 11.4 %all-to-all-start.1 = ((bf16[8,1,2,128,32]{3,4,2,1,0:T(8,128)(2,1)}), bf16[8,1,2,128,32]{3,4,2,1,0:T(8,128)(2,1)S(1)}, u32[]{:S(2)}, u32[]{:S(2)}) async-start(bf16[8,1,2,128,32]{3,4,2,1,0:T(8,128)(2,1)} %constant_dynamic-update-slice_fusion), calls=%async_computation.1 | async-start | bytes 262144 | tf_op jit(solution)/shard_map/all_to_all | solution.py:66
  51.6 93.1 %reduce-scatter.2.cloned.1.call-start = ((), (), s32[]{:S(2)}) async-start(), calls=%async_computation.5 | async-start | bytes 1310720 | tf_op jit(solution)/shard_map/reduce_scatter | solution.py:97
  51.7 15.8 %collective-permute-start = (bf16[2,512]{1,0:T(2,128)(2,1)S(1)}, bf16[2,512]{1,0:T(2,128)(2,1)S(1)}, u32[]{:S(2)}, u32[]{:S(2)}) collective-permute-start(bf16[2,512]{1,0:T(2,128)(2,1)S(1)} %slice.198), channel_id=1, source_target_pairs={{0,4},{4,8},{8,12},{12,16},{16,20},{20,24},{24,28},{1,5},{5,9},{9,... | collective-permute-start | bytes 6152 | tf_op jit(solution)/shard_map/ppermute | solution.py:20
  59.6 0.7 copy-start.8
  65.1 53.0 %copy-start.2 = (bf16[256,512]{1,0:T(8,128)(2,1)S(1)}, bf16[256,512]{1,0:T(8,128)(2,1)}, u32[]{:S(2)}) copy-start(bf16[256,512]{1,0:T(8,128)(2,1)} %param.20) | copy-start | bytes 786436
Sparse Core Ops, SparseCore 0:
  9.4 55.7 all-gather.2
  67.2 50.9 all-gather.4
  121.7 22.9 reduce-scatter.1
